TPU v7x, 32 devices: a whole 2x2x4 slice. The times are simulated.
32 devices in a mesh: ep: 8 (over z, x), tp: 4 (over y, core).
Axes of the slice: x: 2, y: 2, z: 4, core: 2. Of those that a mesh axis runs over, the one named last changes fastest.
Arguments:
- out_gate: bfloat16 [8192, 1024], P('ep', 'tp'), may hold values from -6 to 6
- in_gate: bfloat16 [8192, 1024], P('ep', 'tp'), may hold values from -6 to 6
- conv_input: bfloat16 [8192, 1024], P('ep', 'tp'), may hold values from -6 to 6
- conv_taps: float32 [3, 1024], P(None, 'tp'), may hold values from -4 to 4
- group_gain: float32 [1024], P('tp'), may hold values from 0.1 to 1.9
- mix_out_w: bfloat16 [1024, 2048], replicated, may hold values from -0.1875 to 0.1875
- moe_in: bfloat16 [8192, 2048], P(('ep', 'tp')), may hold values from -6 to 6
- moe_gain: float32 [2048], replicated, may hold values from 0.1 to 1.9
- route_ids: int32 [8192, 2], P(('ep', 'tp')), may hold values from 0 to 31, as said below
- route_weight: float32 [8192, 2], P(('ep', 'tp')), may hold values from 0.1 to 1
- gate_w: bfloat16 [32, 2048, 1024], P(('ep', 'tp')), may hold values from -0.125 to 0.125
- up_w: bfloat16 [32, 2048, 1024], P(('ep', 'tp')), may hold values from -0.125 to 0.125
- down_w: bfloat16 [32, 1024, 2048], P(('ep', 'tp')), may hold values from -0.1875 to 0.1875
Outputs:
- mixed: bfloat16 [8192, 2048], P(('ep', 'tp'))
- moe_out: bfloat16 [8192, 2048], P(('ep', 'tp'))
Inputs may be any that keep to these rules, and one draw needn't show every extreme that they name: `route_ids`: the two numbers of a row are different experts of one group: group g holds experts g * 4 to g * 4 + 3. The rows of one device (aligned blocks of 256 rows) name each group in exactly 32 rows and each expert in exactly 16 rows.
All inputs are finite; a program needn't handle non-finite values.
Results may differ from a plain program's by a relative error of at most 0.0071.
Values may be sent and summed in bfloat16 or wider, within the bound.
A program may use at most 128 MiB of HBM per device.

v0:
```python
import functools

import jax
import jax.numpy as jnp
from jax import lax
from jax.experimental import pallas as pl
from jax.experimental.pallas import tpu as pltpu
from jax.sharding import PartitionSpec as P

GROUP_CH = 64
HALO = 16
MESH = pl.DeviceIdType.MESH
BF16 = jnp.bfloat16
F32 = jnp.float32


def round_up(value, to):
    return (value + to - 1) // to * to


def tdot(a, b):
    return lax.dot_general(a, b, (((0,), (0,)), ((), ())), preferred_element_type=F32)


def dot_t(a, b):
    return lax.dot_general(a, b, (((1,), (1,)), ((), ())), preferred_element_type=F32)


def flip(index, mask):
    bit = 1
    out = index
    while bit <= mask:
        if mask & bit:
            out = out + bit * (1 - 2 * ((index // bit) % 2))
        bit *= 2
    return out


def layer_kernel(
    n_ep, n_tp, pad_slot, chunks, reach,
    og_hbm, ig_hbm, ci_hbm, taps_hbm, ggain_hbm, wm_hbm,
    x_hbm, mgain_hbm, ids_hbm, rw_hbm, wg_hbm, wu_hbm, wd_hbm,
    mixed_hbm, fin_hbm, place_hbm,
    og, ig, ci, taps, ggain, wm, x, mgain, ids, rw, wg, wu, wd,
    normed, gated, norm, place, sorted_rows, landed, picked, xin, hidden, comb, sums, fin, mixin, mixed,
    in_sem, out_sem, h_send, h_recv, m_send, m_recv, d_send, d_recv, p_send, p_recv, r_send, r_recv, f_send, f_recv,
):
    me_e = lax.axis_index("ep")
    me_t = lax.axis_index("tp")
    tok, width = x.shape
    rows = tok // n_ep
    slots = n_tp * pad_slot
    experts = n_ep * n_tp
    rows_a, lanes = og.shape
    part = rows_a // n_tp

    barrier = pltpu.get_barrier_semaphore()
    for k in range(1, n_ep):
        pl.semaphore_signal(
            barrier, inc=1, device_id={"ep": flip(me_e, k), "tp": me_t}, device_id_type=MESH
        )
    for j in range(1, n_tp):
        pl.semaphore_signal(
            barrier, inc=1, device_id={"ep": me_e, "tp": flip(me_t, j)}, device_id_type=MESH
        )
    nxt = lax.rem(me_e + 1, n_ep)
    own = pl.ds(HALO, rows_a)
    loads = {}
    for i, (name, src, dst) in enumerate((
        ("ids", ids_hbm, ids), ("rw", rw_hbm, rw), ("mgain", mgain_hbm, mgain), ("x", x_hbm, x),
        ("ig", ig_hbm, ig.at[own]), ("ci", ci_hbm, ci.at[own]), ("og", og_hbm, og),
        ("taps", taps_hbm, taps), ("ggain", ggain_hbm, ggain),
        ("wg", wg_hbm.at[0], wg), ("wu", wu_hbm.at[0], wu), ("wd", wd_hbm.at[0], wd), ("wm", wm_hbm, wm),
    )):
        loads[name] = pltpu.make_async_copy(src, dst, in_sem.at[i])
        loads[name].start()

    loads["ids"].wait()
    loads["rw"].wait()
    ids0, ids1 = ids[0:1, :], ids[1:2, :]
    sub_e = lax.broadcasted_iota(jnp.int32, (experts, tok), 0)
    hit0 = (ids0 == sub_e).astype(F32)
    hit1 = (ids1 == sub_e).astype(F32)
    both = (hit0 + hit1).astype(BF16)
    upper = (
        lax.broadcasted_iota(jnp.int32, (tok, tok), 0) < lax.broadcasted_iota(jnp.int32, (tok, tok), 1)
    ).astype(BF16)
    before = jnp.dot(both, upper, preferred_element_type=F32)
    rank0 = jnp.sum(before * hit0, axis=0, keepdims=True).astype(jnp.int32)
    rank1 = jnp.sum(before * hit1, axis=0, keepdims=True).astype(jnp.int32)
    group = ids0 // n_tp
    in_group = (group == (sub_e // n_tp)).astype(F32)
    rank_g = jnp.sum(before * in_group, axis=0, keepdims=True).astype(jnp.int32) // 2
    place[...] = (
        (group * rows + rank_g) == lax.broadcasted_iota(jnp.int32, (tok, tok), 0)
    ).astype(BF16)
    place_out = pltpu.make_async_copy(place, place_hbm, out_sem.at[0])
    place_out.start()
    cell0 = (ids0 - group * n_tp) * pad_slot + rank0
    cell1 = (ids1 - group * n_tp) * pad_slot + rank1
    sub_s = lax.broadcasted_iota(jnp.int32, (slots, tok), 0)
    weight = jnp.where(cell0 == sub_s, rw[0:1, :], 0.0) + jnp.where(cell1 == sub_s, rw[1:2, :], 0.0)
    high = weight.astype(BF16)
    low = (weight - high.astype(F32)).astype(BF16)
    cells = jnp.concatenate([high, low], axis=0)
    sorted_rows[:, width:] = dot_t(place[...], cells).astype(BF16)

    loads["mgain"].wait()
    loads["x"].wait()
    step = 32

    @pl.loop(0, tok // step)
    def _(i):
        at = pl.ds(pl.multiple_of(i * step, step), step)
        wide = x[at, :].astype(F32)
        scale = lax.rsqrt(jnp.mean(wide * wide, axis=-1, keepdims=True) + 1e-06)
        norm[at, :] = (wide * scale * mgain[...]).astype(BF16)

    @pl.loop(0, width // 512)
    def _(f):
        cols = pl.ds(pl.multiple_of(f * 512, 512), 512)
        sorted_rows[:, cols] = jnp.dot(
            place[...], norm[:, cols], preferred_element_type=F32
        ).astype(BF16)

    pl.semaphore_wait(barrier, n_ep - 1 + n_tp - 1)

    sends = []

    def send(src, dst, s_sem, r_sem, ep, tp):
        copy = pltpu.make_async_remote_copy(
            src_ref=src, dst_ref=dst, send_sem=s_sem, recv_sem=r_sem,
            device_id={"ep": ep, "tp": tp}, device_id_type=MESH,
        )
        copy.start()
        sends.append(copy)
        return copy

    dispatch = {}
    for k in range(1, n_ep):
        to = flip(me_e, k)
        dispatch[k] = send(
            sorted_rows.at[pl.ds(pl.multiple_of(to * rows, rows), rows)],
            landed.at[k], d_send.at[k], d_recv.at[k], to, me_t,
        )
    loads["ig"].wait()
    loads["ci"].wait()
    tail, head = pl.ds(rows_a, HALO), pl.ds(0, HALO)
    halos = [
        send(ref.at[tail], ref.at[head], h_send.at[i], h_recv.at[i], nxt, me_t)
        for i, ref in enumerate((ig, ci))
    ]
    landed[0] = sorted_rows[pl.ds(pl.multiple_of(me_e * rows, rows), rows), :]

    spread = {}

    def scatter(k):
        if k:
            dispatch[k].wait_recv()
        chosen = (landed[k, :, pl.ds(width, slots)].astype(F32) != 0.0).astype(BF16)
        picked[k] = tdot(chosen, landed[k, :, 0:width]).astype(BF16)
        for j in range(n_tp - 1, 0, -1):
            to = flip(me_t, j)
            spread[k, j] = send(
                picked.at[k, pl.ds(pl.multiple_of(to * pad_slot, pad_slot), pad_slot)],
                xin.at[pl.ds((k * n_tp + j) * pad_slot, pad_slot)],
                p_send.at[k, j], p_recv.at[k, j], me_e, to,
            )
        xin[pl.ds(k * n_tp * pad_slot, pad_slot), :] = picked[
            k, pl.ds(pl.multiple_of(me_t * pad_slot, pad_slot), pad_slot), :
        ]

    scatter(0)

    loads["og"].wait()
    loads["taps"].wait()
    loads["ggain"].wait()
    for copy in halos:
        copy.wait_recv()

    @pl.when(me_e == 0)
    def _():
        ig[0:HALO, :] = jnp.zeros((HALO, lanes), BF16)

    same = (
        lax.broadcasted_iota(jnp.int32, (lanes, lanes), 0) // GROUP_CH
        == lax.broadcasted_iota(jnp.int32, (lanes, lanes), 1) // GROUP_CH
    ).astype(BF16)
    own_lanes = pl.ds(pl.multiple_of(me_t * lanes, lanes), lanes)
    mixes = []
    for j in range(n_tp - 1, -1, -1):
        to = flip(me_t, j)
        base = pl.multiple_of(to * part, part)
        cstep = 64

        @pl.loop(0, part // cstep)
        def _(i):
            at = pl.multiple_of(base + i * cstep, cstep)
            span = pl.ds(at, cstep + HALO)
            product = ig[span, :].astype(F32) * ci[span, :].astype(F32)
            total = taps[reach : reach + 1, :] * product[HALO:, :]
            for back_by in range(1, reach + 1):
                total = total + taps[reach - back_by : reach - back_by + 1, :] * (
                    product[HALO - back_by : HALO - back_by + cstep, :]
                )
            gated[pl.ds(pl.multiple_of(i * cstep, cstep), cstep), :] = (
                og[pl.ds(at, cstep), :].astype(F32) * total
            )

        value = gated[...]
        square = value * value
        s_high = square.astype(BF16)
        s_low = (square - s_high.astype(F32)).astype(BF16)
        mean = (
            jnp.dot(s_high, same, preferred_element_type=F32)
            + jnp.dot(s_low, same, preferred_element_type=F32)
        ) * (1.0 / GROUP_CH)
        done = (value * lax.rsqrt(mean + 1e-06) * ggain[...]).astype(BF16)
        if j:
            normed[pl.ds(base, part), :] = done
            mixes.append(send(
                normed.at[pl.ds(base, part)], mixin.at[:, own_lanes],
                m_send.at[j], m_recv.at[j], me_e, to,
            ))
        else:
            mixin[:, own_lanes] = done

    hid = wg.shape[1]
    per = n_ep // chunks
    many = per * slots
    back = {}
    mine = pl.ds(pl.multiple_of(me_t * pad_slot, pad_slot), pad_slot)
    here = pl.ds(pl.multiple_of(me_e * rows, rows), rows)

    def expert(c):
        for k in range(c * per, (c + 1) * per):
            for j in range(1, n_tp):
                spread[k, j].wait_recv()
        span = pl.ds(c * many, many)

        @pl.loop(0, hid // 256)
        def _(f):
            cols = pl.ds(pl.multiple_of(f * 256, 256), 256)
            gate = jnp.dot(xin[span, :], wg[:, cols], preferred_element_type=F32)
            up = jnp.dot(xin[span, :], wu[:, cols], preferred_element_type=F32)
            hidden[:, cols] = (gate / (1.0 + jnp.exp(-gate)) * up).astype(BF16)

        @pl.loop(0, width // 512)
        def _(f):
            cols = pl.ds(pl.multiple_of(f * 512, 512), 512)
            xin[span, cols] = jnp.dot(
                hidden[...], wd[:, cols], preferred_element_type=F32
            ).astype(BF16)

    def give_back(c):
        for k in range(c * per, (c + 1) * per):
            for j in range(n_tp - 1, 0, -1):
                back[k, j] = send(
                    xin.at[pl.ds((k * n_tp + j) * pad_slot, pad_slot)],
                    comb.at[k, mine], r_send.at[k, j], r_recv.at[k, j], me_e, flip(me_t, j),
                )
            comb[k, mine, :] = xin[pl.ds(k * slots, pad_slot), :]

    home = {}

    def combine(k):
        for j in range(1, n_tp):
            back[k, j].wait_recv()
        total = jnp.dot(
            landed[k, :, pl.ds(width, slots)], comb[k], preferred_element_type=F32
        ) + jnp.dot(
            landed[k, :, pl.ds(width + slots, slots)], comb[k], preferred_element_type=F32
        )
        if k == 0:
            fin[here, :] = total.astype(BF16)
            return
        sums[k] = total.astype(BF16)
        home[k] = send(sums.at[k], fin.at[here], f_send.at[k], f_recv.at[k], flip(me_e, k), me_t)

    half = n_ep // 2
    near = list(range(chunks // 2))
    far = list(range(chunks // 2, chunks))
    for k in range(1, half):
        scatter(k)
    for name in ("wg", "wu", "wd", "wm"):
        loads[name].wait()
    expert(near[0])
    scatter(half)
    for c in near[1:]:
        expert(c)
    scatter(half + 1)
    for copy in mixes:
        copy.wait_recv()

    @pl.loop(0, width // 512)
    def _(f):
        cols = pl.ds(pl.multiple_of(f * 512, 512), 512)
        mixed[:, cols] = jnp.dot(mixin[...], wm[:, cols], preferred_element_type=F32).astype(BF16)

    mixed_out = pltpu.make_async_copy(mixed, mixed_hbm, out_sem.at[1])
    mixed_out.start()
    for k in range(half + 2, n_ep):
        scatter(k)
    for c in far:
        expert(c)
        give_back(c)
    for c in near[::-1]:
        give_back(c)
    order = [k for c in far + near[::-1] for k in range(c * per, (c + 1) * per)]
    for k in order:
        combine(k)
    fin_out = []

    def finish(k):
        block = pl.ds(pl.multiple_of(flip(me_e, k) * rows, rows), rows)
        copy = pltpu.make_async_copy(fin.at[block], fin_hbm.at[block], out_sem.at[2 + k])
        copy.start()
        fin_out.append(copy)

    for k in order:
        if k:
            home[k].wait_recv()
        finish(k)
    for copy in sends:
        copy.wait_send()
    for copy in [place_out, mixed_out] + fin_out:
        copy.wait()


def layer(
    out_gate, in_gate, conv_input, conv_taps, group_gain, mix_out_w,
    moe_in, moe_gain, route_ids, route_weight, gate_w, up_w, down_w,
):
    n_ep, n_tp = lax.axis_size("ep"), lax.axis_size("tp")
    tok, width = moe_in.shape
    hid = gate_w.shape[2]
    pad_slot = round_up(2 * tok // (n_ep * n_tp), 16)
    rows = tok // n_ep
    slots = n_tp * pad_slot
    meta = round_up(2 * slots, 128)
    total = n_ep * slots
    chunks = 4
    rows_a, lanes = out_gate.shape
    part = rows_a // n_tp
    channels = mix_out_w.shape[0]
    taps = conv_taps.shape[0]
    hbm = pl.BlockSpec(memory_space=pl.ANY)
    dma = pltpu.SemaphoreType.DMA
    vm = pltpu.VMEM
    return pl.pallas_call(
        functools.partial(layer_kernel, n_ep, n_tp, pad_slot, chunks, taps - 1),
        out_shape=[
            jax.ShapeDtypeStruct((part, width), BF16),
            jax.ShapeDtypeStruct((tok, width), BF16),
            jax.ShapeDtypeStruct((tok, tok), BF16),
        ],
        in_specs=[hbm] * 13,
        out_specs=[hbm] * 3,
        scratch_shapes=[
            vm((rows_a, lanes), BF16),
            vm((HALO + rows_a, lanes), BF16),
            vm((HALO + rows_a, lanes), BF16),
            vm((taps, lanes), F32),
            vm((1, lanes), F32),
            vm((channels, width), BF16),
            vm((tok, width), BF16),
            vm((1, width), F32),
            vm((2, tok), jnp.int32),
            vm((2, tok), F32),
            vm((width, hid), BF16),
            vm((width, hid), BF16),
            vm((hid, width), BF16),
            vm((rows_a, lanes), BF16),
            vm((part, lanes), F32),
            vm((tok, width), BF16),
            vm((tok, tok), BF16),
            vm((tok, width + meta), BF16),
            vm((n_ep, rows, width + meta), BF16),
            vm((n_ep, slots, width), BF16),
            vm((total, width), BF16),
            vm((total // chunks, hid), BF16),
            vm((n_ep, slots, width), BF16),
            vm((n_ep, rows, width), BF16),
            vm((tok, width), BF16),
            vm((part, channels), BF16),
            vm((part, width), BF16),
            dma((13,)),
            dma((2 + n_ep,)),
            dma((2,)),
            dma((2,)),
            dma((n_tp,)),
            dma((n_tp,)),
            dma((n_ep,)),
            dma((n_ep,)),
            dma((n_ep, n_tp)),
            dma((n_ep, n_tp)),
            dma((n_ep, n_tp)),
            dma((n_ep, n_tp)),
            dma((n_ep,)),
            dma((n_ep,)),
        ],
        compiler_params=pltpu.CompilerParams(
            collective_id=0, has_side_effects=True, vmem_limit_bytes=60 * 1024 * 1024
        ),
        cost_estimate=pl.CostEstimate(
            flops=6 * total * width * hid, bytes_accessed=8 * width * hid, transcendentals=0
        ),
    )(
        out_gate, in_gate, conv_input, conv_taps, group_gain.reshape(1, lanes), mix_out_w,
        moe_in, moe_gain.reshape(1, width), route_ids.T, route_weight.T, gate_w, up_w, down_w,
    )


def finish_kernel(mixed_in, fin, place, mixed, out):
    mixed[...] = mixed_in[...]
    out[...] = tdot(place[...], fin[...]).astype(BF16)


def shards(*args):
    mixed, fin, place = layer(*args)
    tok, width = fin.shape
    block = 512
    cols = lambda rows: pl.BlockSpec((rows, block), lambda i: (0, i))
    return pl.pallas_call(
        finish_kernel,
        grid=(width // block,),
        out_shape=[
            jax.ShapeDtypeStruct(mixed.shape, BF16),
            jax.ShapeDtypeStruct((tok, width), BF16),
        ],
        in_specs=[cols(mixed.shape[0]), cols(tok), pl.BlockSpec((tok, tok), lambda i: (0, 0))],
        out_specs=[cols(mixed.shape[0]), cols(tok)],
        cost_estimate=pl.CostEstimate(
            flops=2 * tok * tok * width, bytes_accessed=8 * tok * width, transcendentals=0
        ),
    )(mixed, fin, place)


def solution(mesh):
    in_specs = (
        P("ep", "tp"),
        P("ep", "tp"),
        P("ep", "tp"),
        P(None, "tp"),
        P("tp"),
        P(),
        P(("ep", "tp"), None),
        P(),
        P(("ep", "tp"), None),
        P(("ep", "tp"), None),
        P(("ep", "tp"), None, None),
        P(("ep", "tp"), None, None),
        P(("ep", "tp"), None, None),
    )
    out_specs = (P(("ep", "tp"), None), P(("ep", "tp"), None))
    return jax.shard_map(shards, mesh=mesh, in_specs=in_specs, out_specs=out_specs, check_vma=False)
```

profile of v0, /device:TPU:18, one launch (start us, length us, event | category | flops | bytes accessed | tf_op | source)
XLA Modules:
  0.0 92.3 jit_solution(4313923833601225756)
XLA Ops:
  0.6 87.6 %shard_map.140 = (bf16[256,2048]{1,0:T(8,128)(2,1)}, bf16[256,2048]{1,0:T(8,128)(2,1)}, bf16[256,256]{1,0:T(8,128)(2,1)}) custom-call(bf16[1024,256]{1,0:T(8,128)(2,1)} %og_hbm.1, bf16[1024,256]{1,0:T(8,128)(2,1)} %ig_hbm.1, bf16[1024,256]{1,0:T(8,128)(2,1)} %ci_hbm.1, f32[3,256]{1,0:T(4,128)} %taps_hbm.1, f32[1,256]{1,0:T(1,128)} %bitcast.7, ...), custom_call_target="tpu_custom_call" | custom-call | flops 6442450944 | bytes 16777216 | tf_op jit(solution)/shard_map/pallas_call | solution.py:350
  88.3 4.1 %shard_map.141 = (bf16[256,2048]{1,0:T(8,128)(2,1)}, bf16[256,2048]{1,0:T(8,128)(2,1)}) custom-call(bf16[256,2048]{1,0:T(8,128)(2,1)} %get-tuple-element.5.mixed_in, bf16[256,2048]{1,0:T(8,128)(2,1)} %get-tuple-element.6.fin, bf16[256,256]{1,0:T(8,128)(2,1)} %get-tuple-element.7.place), custom_call_target="tpu_custom_call" | custom-call | flops 268435456 | bytes 4194304 | tf_op jit(solution)/shard_map/pallas_call | solution.py:424
where the time goes:
time: 92.5 us; the launch traced here: 92.3 us
  Pallas kernels  91.7 us (99%)
    pallas_call x1, Pallas kernels, layer(): pl.pallas_call(functools.partial(layer_kernel, n_ep, n_tp, pad_slot, chun...  87.6 us
    pallas_call x1, Pallas kernels, shards(): pl.pallas_call(finish_kernel, grid=(width // block,), out_shape=[jax.Shap...  4.08 us

commit v1 on v0

--- a/solution.py
+++ b/solution.py
@@ -136,6 +136,13 @@
         sends.append(copy)
         return copy
 
+    loads["ig"].wait()
+    loads["ci"].wait()
+    tail, head = pl.ds(rows_a, HALO), pl.ds(0, HALO)
+    halos = [
+        send(ref.at[tail], ref.at[head], h_send.at[i], h_recv.at[i], nxt, me_t)
+        for i, ref in enumerate((ig, ci))
+    ]
     dispatch = {}
     for k in range(1, n_ep):
         to = flip(me_e, k)
@@ -143,13 +150,6 @@
             sorted_rows.at[pl.ds(pl.multiple_of(to * rows, rows), rows)],
             landed.at[k], d_send.at[k], d_recv.at[k], to, me_t,
         )
-    loads["ig"].wait()
-    loads["ci"].wait()
-    tail, head = pl.ds(rows_a, HALO), pl.ds(0, HALO)
-    halos = [
-        send(ref.at[tail], ref.at[head], h_send.at[i], h_recv.at[i], nxt, me_t)
-        for i, ref in enumerate((ig, ci))
-    ]
     landed[0] = sorted_rows[pl.ds(pl.multiple_of(me_e * rows, rows), rows), :]
 
     spread = {}

time: 92.5 us -> 75.5 us (0.82)
  the two profiles are of different devices: /device:TPU:18 before, /device:TPU:0 now
where the time goes in v1:
time: 75.5 us; the launch traced here: 75.3 us
  Pallas kernels  74.7 us (99%)
    pallas_call x1, Pallas kernels, layer(): pl.pallas_call(functools.partial(layer_kernel, n_ep, n_tp, pad_slot, chun...  70.6 us
    pallas_call x1, Pallas kernels, shards(): pl.pallas_call(finish_kernel, grid=(width // block,), out_shape=[jax.Shap...  4.08 us

profile of v1, /device:TPU:0, one launch (start us, length us, event | category | flops | bytes accessed | tf_op | source)
XLA Modules:
  0.0 75.3 jit_solution(1885927026790281373)
XLA Ops:
  0.6 70.6 %shard_map.140 = (bf16[256,2048]{1,0:T(8,128)(2,1)}, bf16[256,2048]{1,0:T(8,128)(2,1)}, bf16[256,256]{1,0:T(8,128)(2,1)}) custom-call(bf16[1024,256]{1,0:T(8,128)(2,1)} %og_hbm.1, bf16[1024,256]{1,0:T(8,128)(2,1)} %ig_hbm.1, bf16[1024,256]{1,0:T(8,128)(2,1)} %ci_hbm.1, f32[3,256]{1,0:T(4,128)} %taps_hbm.1, f32[1,256]{1,0:T(1,128)} %bitcast.7, ...), custom_call_target="tpu_custom_call" | custom-call | flops 6442450944 | bytes 16777216 | tf_op jit(solution)/shard_map/pallas_call | solution.py:350
  71.2 4.1 %shard_map.141 = (bf16[256,2048]{1,0:T(8,128)(2,1)}, bf16[256,2048]{1,0:T(8,128)(2,1)}) custom-call(bf16[256,2048]{1,0:T(8,128)(2,1)} %get-tuple-element.5.mixed_in, bf16[256,2048]{1,0:T(8,128)(2,1)} %get-tuple-element.6.fin, bf16[256,256]{1,0:T(8,128)(2,1)} %get-tuple-element.7.place), custom_call_target="tpu_custom_call" | custom-call | flops 268435456 | bytes 4194304 | tf_op jit(solution)/shard_map/pallas_call | solution.py:424

commit v2 on v1

v2 whole, which is shorter than its diff:
```python
import functools
import math

import jax
import jax.numpy as jnp
from jax import lax
from jax.experimental import pallas as pl
from jax.experimental.pallas import tpu as pltpu
from jax.sharding import PartitionSpec as P

GROUP_CH = 64
HALO = 16
VMEM_BYTES = 60 * 1024 * 1024
SPARE = 6 << 20
MESH = pl.DeviceIdType.MESH
BF16 = jnp.bfloat16
F32 = jnp.float32


def round_up(value, to):
    return (value + to - 1) // to * to


def tdot(a, b):
    return lax.dot_general(a, b, (((0,), (0,)), ((), ())), preferred_element_type=F32)


def dot_t(a, b):
    return lax.dot_general(a, b, (((1,), (1,)), ((), ())), preferred_element_type=F32)


def flip(index, mask):
    bit = 1
    out = index
    while bit <= mask:
        if mask & bit:
            out = out + bit * (1 - 2 * ((index // bit) % 2))
        bit *= 2
    return out


def layer_kernel(
    n_ep, n_tp, pad_slot, reach,
    og_hbm, ig_hbm, ci_hbm, taps_hbm, ggain_hbm, wm_hbm,
    x_hbm, mgain_hbm, ids_hbm, rw_hbm, wg_hbm, wu_hbm, wd_hbm,
    mixed, fin, place,
    og, ig, ci, taps, ggain, wm, x, mgain, ids, rw, wg, wu, wd,
    normed, gated, norm, sorted_rows, landed, picked, xin, hidden, comb, sums, mixin,
    in_sem, h_send, h_recv, m_send, m_recv, d_send, d_recv, p_send, p_recv, r_send, r_recv, f_send, f_recv,
):
    me_e = lax.axis_index("ep")
    me_t = lax.axis_index("tp")
    tok, width = x.shape
    rows = tok // n_ep
    slots = n_tp * pad_slot
    experts = n_ep * n_tp
    rows_a, lanes = og.shape
    part = rows_a // n_tp
    quarter = n_ep // 4

    barrier = pltpu.get_barrier_semaphore()
    for k in range(1, n_ep):
        pl.semaphore_signal(
            barrier, inc=1, device_id={"ep": flip(me_e, k), "tp": me_t}, device_id_type=MESH
        )
    for j in range(1, n_tp):
        pl.semaphore_signal(
            barrier, inc=1, device_id={"ep": me_e, "tp": flip(me_t, j)}, device_id_type=MESH
        )
    nxt = lax.rem(me_e + 1, n_ep)
    own = pl.ds(HALO, rows_a)
    loads = {}
    for i, (name, src, dst) in enumerate((
        ("ids", ids_hbm, ids), ("rw", rw_hbm, rw), ("mgain", mgain_hbm, mgain), ("x", x_hbm, x),
        ("ig", ig_hbm, ig.at[own]), ("ci", ci_hbm, ci.at[own]), ("og", og_hbm, og),
        ("taps", taps_hbm, taps), ("ggain", ggain_hbm, ggain),
        ("wg", wg_hbm.at[0], wg), ("wu", wu_hbm.at[0], wu), ("wd", wd_hbm.at[0], wd), ("wm", wm_hbm, wm),
    )):
        loads[name] = pltpu.make_async_copy(src, dst, in_sem.at[i])
        loads[name].start()

    loads["ids"].wait()
    loads["rw"].wait()
    ids0, ids1 = ids[0:1, :], ids[1:2, :]
    sub_e = lax.broadcasted_iota(jnp.int32, (experts, tok), 0)
    hit0 = (ids0 == sub_e).astype(F32)
    hit1 = (ids1 == sub_e).astype(F32)
    both = (hit0 + hit1).astype(BF16)
    upper = (
        lax.broadcasted_iota(jnp.int32, (tok, tok), 0) < lax.broadcasted_iota(jnp.int32, (tok, tok), 1)
    ).astype(BF16)
    before = jnp.dot(both, upper, preferred_element_type=F32)
    rank0 = jnp.sum(before * hit0, axis=0, keepdims=True).astype(jnp.int32)
    rank1 = jnp.sum(before * hit1, axis=0, keepdims=True).astype(jnp.int32)
    group = ids0 // n_tp
    in_group = (group == (sub_e // n_tp)).astype(F32)
    rank_g = jnp.sum(before * in_group, axis=0, keepdims=True).astype(jnp.int32) // 2
    place[...] = (
        (group * rows + rank_g) == lax.broadcasted_iota(jnp.int32, (tok, tok), 0)
    ).astype(BF16)
    cell0 = (ids0 - group * n_tp) * pad_slot + rank0
    cell1 = (ids1 - group * n_tp) * pad_slot + rank1
    sub_s = lax.broadcasted_iota(jnp.int32, (slots, tok), 0)
    weight = jnp.where(cell0 == sub_s, rw[0:1, :], 0.0) + jnp.where(cell1 == sub_s, rw[1:2, :], 0.0)
    high = weight.astype(BF16)
    low = (weight - high.astype(F32)).astype(BF16)
    cells = jnp.concatenate([high, low], axis=0)
    sorted_rows[:, width:] = dot_t(place[...], cells).astype(BF16)

    loads["mgain"].wait()
    loads["x"].wait()
    step = 32

    @pl.loop(0, tok // step)
    def _(i):
        at = pl.ds(pl.multiple_of(i * step, step), step)
        wide = x[at, :].astype(F32)
        scale = lax.rsqrt(jnp.mean(wide * wide, axis=-1, keepdims=True) + 1e-06)
        norm[at, :] = (wide * scale * mgain[...]).astype(BF16)

    @pl.loop(0, width // 512)
    def _(f):
        cols = pl.ds(pl.multiple_of(f * 512, 512), 512)
        sorted_rows[:, cols] = jnp.dot(
            place[...], norm[:, cols], preferred_element_type=F32
        ).astype(BF16)

    pl.semaphore_wait(barrier, n_ep - 1 + n_tp - 1)

    others = pl.ds(0, (n_tp - 1) * pad_slot)

    def settle(sem, like):
        pltpu.make_async_copy(like, like, sem).wait()

    def send(src, dst, s_sem, r_sem, ep, tp):
        copy = pltpu.make_async_remote_copy(
            src_ref=src, dst_ref=dst, send_sem=s_sem, recv_sem=r_sem,
            device_id={"ep": ep, "tp": tp}, device_id_type=MESH,
        )
        copy.start()
        return copy

    loads["ig"].wait()
    loads["ci"].wait()
    tail, head = pl.ds(rows_a, HALO), pl.ds(0, HALO)
    halos = [
        pltpu.make_async_remote_copy(
            src_ref=ref.at[tail], dst_ref=ref.at[head], send_sem=h_send, recv_sem=h_recv,
            device_id={"ep": nxt, "tp": me_t}, device_id_type=MESH,
        )
        for ref in (ig, ci)
    ]

    @pl.when(me_e < n_ep - 1)
    def _():
        for copy in halos:
            copy.start()

    dispatch = {}
    for k in range(1, n_ep):
        to = flip(me_e, k)
        dispatch[k] = send(
            sorted_rows.at[pl.ds(pl.multiple_of(to * rows, rows), rows)],
            landed.at[k], d_send, d_recv.at[k], to, me_t,
        )
    landed[0] = sorted_rows[pl.ds(pl.multiple_of(me_e * rows, rows), rows), :]

    def scatter(k):
        if k:
            dispatch[k].wait_recv()
        chosen = (landed[k, :, pl.ds(width, slots)].astype(F32) != 0.0).astype(BF16)
        picked[k] = tdot(chosen, landed[k, :, 0:width]).astype(BF16)
        for j in range(n_tp - 1, 0, -1):
            to = flip(me_t, j)
            send(
                picked.at[k, pl.ds(pl.multiple_of(to * pad_slot, pad_slot), pad_slot)],
                xin.at[pl.ds((k * n_tp + j) * pad_slot, pad_slot)],
                p_send, p_recv.at[k // quarter], me_e, to,
            )
        xin[pl.ds(k * n_tp * pad_slot, pad_slot), :] = picked[
            k, pl.ds(pl.multiple_of(me_t * pad_slot, pad_slot), pad_slot), :
        ]

    own_lanes = pl.ds(pl.multiple_of(me_t * lanes, lanes), lanes)

    def conv_ready():
        for name in ("og", "taps", "ggain"):
            loads[name].wait()

        @pl.when(me_e > 0)
        def _():
            settle(h_recv, ig.at[pl.ds(0, 2 * HALO)])

        @pl.when(me_e == 0)
        def _():
            ig[0:HALO, :] = jnp.zeros((HALO, lanes), BF16)

    def conv(j):
        same = (
            lax.broadcasted_iota(jnp.int32, (lanes, lanes), 0) // GROUP_CH
            == lax.broadcasted_iota(jnp.int32, (lanes, lanes), 1) // GROUP_CH
        ).astype(BF16)
        base = pl.multiple_of(flip(me_t, j) * part, part)
        cstep = 64

        @pl.loop(0, part // cstep)
        def _(i):
            at = pl.multiple_of(base + i * cstep, cstep)
            span = pl.ds(at, cstep + HALO)
            product = ig[span, :].astype(F32) * ci[span, :].astype(F32)
            total = taps[reach : reach + 1, :] * product[HALO:, :]
            for back_by in range(1, reach + 1):
                total = total + taps[reach - back_by : reach - back_by + 1, :] * (
                    product[HALO - back_by : HALO - back_by + cstep, :]
                )
            gated[pl.ds(pl.multiple_of(i * cstep, cstep), cstep), :] = (
                og[pl.ds(at, cstep), :].astype(F32) * total
            )

        value = gated[...]
        square = value * value
        s_high = square.astype(BF16)
        s_low = (square - s_high.astype(F32)).astype(BF16)
        mean = (
            jnp.dot(s_high, same, preferred_element_type=F32)
            + jnp.dot(s_low, same, preferred_element_type=F32)
        ) * (1.0 / GROUP_CH)
        done = (value * lax.rsqrt(mean + 1e-06) * ggain[...]).astype(BF16)
        if j:
            normed[pl.ds(base, part), :] = done
        else:
            mixin[:, own_lanes] = done

    def mix_send(j):
        to = flip(me_t, j)
        send(
            normed.at[pl.ds(pl.multiple_of(to * part, part), part)], mixin.at[:, own_lanes],
            m_send, m_recv, me_e, to,
        )

    def mixer():
        settle(m_recv, mixin.at[:, pl.ds(0, (n_tp - 1) * lanes)])

        @pl.loop(0, width // 512)
        def _(f):
            cols = pl.ds(pl.multiple_of(f * 512, 512), 512)
            mixed[:, cols] = jnp.dot(mixin[...], wm[:, cols], preferred_element_type=F32).astype(BF16)

    hid = wg.shape[1]
    mine = pl.ds(pl.multiple_of(me_t * pad_slot, pad_slot), pad_slot)
    here = pl.ds(pl.multiple_of(me_e * rows, rows), rows)

    def expert(first, count):
        settle(p_recv.at[first // quarter], xin.at[pl.ds(first * slots, count * (n_tp - 1) * pad_slot)])
        span = pl.ds(first * slots, count * slots)
        hid_rows = pl.ds(0, count * slots)

        @pl.loop(0, hid // 256)
        def _(f):
            cols = pl.ds(pl.multiple_of(f * 256, 256), 256)
            gate = jnp.dot(xin[span, :], wg[:, cols], preferred_element_type=F32)
            up = jnp.dot(xin[span, :], wu[:, cols], preferred_element_type=F32)
            hidden[hid_rows, cols] = (gate / (1.0 + jnp.exp(-gate)) * up).astype(BF16)

        @pl.loop(0, width // 512)
        def _(f):
            cols = pl.ds(pl.multiple_of(f * 512, 512), 512)
            xin[span, cols] = jnp.dot(
                hidden[hid_rows, :], wd[:, cols], preferred_element_type=F32
            ).astype(BF16)

    def give_back(first, count):
        for k in range(first, first + count):
            for j in range(n_tp - 1, 0, -1):
                send(
                    xin.at[pl.ds((k * n_tp + j) * pad_slot, pad_slot)],
                    comb.at[k, mine], r_send, r_recv.at[k], me_e, flip(me_t, j),
                )
            comb[k, mine, :] = xin[pl.ds(k * slots, pad_slot), :]


    def combine(k):
        settle(r_recv.at[k], comb.at[k, others])
        total = jnp.dot(
            landed[k, :, pl.ds(width, slots)], comb[k], preferred_element_type=F32
        ) + jnp.dot(
            landed[k, :, pl.ds(width + slots, slots)], comb[k], preferred_element_type=F32
        )
        if k == 0:
            fin[here, :] = total.astype(BF16)
            return
        sums[k] = total.astype(BF16)
        send(sums.at[k], fin.at[here], f_send, f_recv, flip(me_e, k), me_t)

    half = n_ep // 2
    scatter(0)
    conv_ready()
    for j in range(n_tp - 1, 0, -1):
        conv(j)
        mix_send(j)
    conv(0)
    for k in range(1, half):
        scatter(k)
    loads["wm"].wait()
    mixer()
    for name in ("wg", "wu", "wd"):
        loads[name].wait()
    for k in range(half, half + quarter):
        scatter(k)
    expert(0, quarter)
    for k in range(half + quarter, n_ep):
        scatter(k)
    expert(half, quarter)
    give_back(half, quarter)
    expert(half + quarter, quarter)
    give_back(half + quarter, quarter)
    for k in range(half, half + quarter):
        combine(k)
    expert(quarter, quarter)
    give_back(quarter, quarter)
    give_back(0, quarter)
    for k in range(half + quarter, n_ep):
        combine(k)
    for k in range(half - 1, quarter - 1, -1):
        combine(k)
    for k in range(quarter - 1, -1, -1):
        combine(k)
    settle(f_recv, fin.at[pl.ds(0, (n_ep - 1) * rows)])
    @pl.when(me_e < n_ep - 1)
    def _():
        settle(h_send, ig.at[pl.ds(0, 2 * HALO)])

    settle(d_send, sorted_rows.at[pl.ds(0, (n_ep - 1) * rows)])
    settle(m_send, normed.at[pl.ds(0, (n_tp - 1) * part)])
    settle(p_send, picked.at[:, others])
    settle(r_send, comb.at[:, others])
    settle(f_send, sums.at[pl.ds(0, n_ep - 1)])


def layer(
    out_gate, in_gate, conv_input, conv_taps, group_gain, mix_out_w,
    moe_in, moe_gain, route_ids, route_weight, gate_w, up_w, down_w,
):
    n_ep, n_tp = lax.axis_size("ep"), lax.axis_size("tp")
    tok, width = moe_in.shape
    hid = gate_w.shape[2]
    pad_slot = round_up(2 * tok // (n_ep * n_tp), 16)
    rows = tok // n_ep
    slots = n_tp * pad_slot
    meta = round_up(2 * slots, 128)
    total = n_ep * slots
    rows_a, lanes = out_gate.shape
    part = rows_a // n_tp
    channels = mix_out_w.shape[0]
    taps = conv_taps.shape[0]
    hbm = pl.BlockSpec(memory_space=pltpu.HBM)
    dma = pltpu.SemaphoreType.DMA
    vm = pltpu.VMEM
    scratch = [
        vm((rows_a, lanes), BF16),
        vm((HALO + rows_a, lanes), BF16),
        vm((HALO + rows_a, lanes), BF16),
        vm((taps, lanes), F32),
        vm((1, lanes), F32),
        vm((channels, width), BF16),
        vm((tok, width), BF16),
        vm((1, width), F32),
        vm((2, tok), jnp.int32),
        vm((2, tok), F32),
        vm((width, hid), BF16),
        vm((width, hid), BF16),
        vm((hid, width), BF16),
        vm((rows_a, lanes), BF16),
        vm((part, lanes), F32),
        vm((tok, width), BF16),
        vm((tok, width + meta), BF16),
        vm((n_ep, rows, width + meta), BF16),
        vm((n_ep, slots, width), BF16),
        vm((total, width), BF16),
        vm((total // 4, hid), BF16),
        vm((n_ep, slots, width), BF16),
        vm((n_ep, rows, width), BF16),
        vm((part, channels), BF16),
        dma((13,)),
        dma(()),
        dma(()),
        dma(()),
        dma(()),
        dma(()),
        dma((n_ep,)),
        dma(()),
        dma((4,)),
        dma(()),
        dma((n_ep,)),
        dma(()),
        dma(()),
    ]
    held = 2 * (part * width + tok * width + tok * tok) + sum(
        math.prod(one.shape) * jnp.dtype(one.dtype).itemsize for one in scratch if one.memory_space == vm
    )
    return pl.pallas_call(
        functools.partial(layer_kernel, n_ep, n_tp, pad_slot, taps - 1),
        out_shape=[
            jax.ShapeDtypeStruct((part, width), BF16),
            jax.ShapeDtypeStruct((tok, width), BF16),
            jax.ShapeDtypeStruct((tok, tok), BF16),
        ],
        in_specs=[hbm] * 13,
        out_specs=[pl.BlockSpec(memory_space=vm)] * 3,
        scratch_shapes=scratch,
        compiler_params=pltpu.CompilerParams(
            collective_id=0, has_side_effects=True, vmem_limit_bytes=min(held + SPARE, VMEM_BYTES)
        ),
        cost_estimate=pl.CostEstimate(
            flops=6 * total * width * hid, bytes_accessed=8 * width * hid, transcendentals=0
        ),
    )(*[pltpu.with_memory_space_constraint(a, pltpu.HBM) for a in (
        out_gate, in_gate, conv_input, conv_taps, group_gain.reshape(1, lanes), mix_out_w,
        moe_in, moe_gain.reshape(1, width), route_ids.T, route_weight.T, gate_w, up_w, down_w,
    )])


def finish_kernel(mixed_in, fin, place, mixed, out, done, sem):
    copies = [pltpu.make_async_copy(mixed_in, mixed, sem.at[0])]
    copies[0].start()
    block = 512
    for i in range(done.shape[1] // block):
        cols = pl.ds(i * block, block)
        done[:, cols] = tdot(place[...], fin[:, cols]).astype(BF16)
        copies.append(pltpu.make_async_copy(done.at[:, cols], out.at[:, cols], sem.at[1 + i]))
        copies[-1].start()
    for copy in copies:
        copy.wait()


def shards(*args):
    mixed, fin, place = layer(*args)
    tok, width = fin.shape
    vm = pl.BlockSpec(memory_space=pltpu.VMEM)
    hbm = pl.BlockSpec(memory_space=pl.ANY)
    return pl.pallas_call(
        finish_kernel,
        out_shape=[
            jax.ShapeDtypeStruct(mixed.shape, BF16),
            jax.ShapeDtypeStruct((tok, width), BF16),
        ],
        in_specs=[vm, vm, vm],
        out_specs=[hbm, hbm],
        scratch_shapes=[pltpu.VMEM((tok, width), BF16), pltpu.SemaphoreType.DMA((1 + width // 512,))],
        compiler_params=pltpu.CompilerParams(vmem_limit_bytes=8 << 20),
        cost_estimate=pl.CostEstimate(
            flops=2 * tok * tok * width, bytes_accessed=8 * tok * width, transcendentals=0
        ),
    )(mixed, fin, place)


def solution(mesh):
    in_specs = (
        P("ep", "tp"),
        P("ep", "tp"),
        P("ep", "tp"),
        P(None, "tp"),
        P("tp"),
        P(),
        P(("ep", "tp"), None),
        P(),
        P(("ep", "tp"), None),
        P(("ep", "tp"), None),
        P(("ep", "tp"), None, None),
        P(("ep", "tp"), None, None),
        P(("ep", "tp"), None, None),
    )
    out_specs = (P(("ep", "tp"), None), P(("ep", "tp"), None))
    return jax.shard_map(shards, mesh=mesh, in_specs=in_specs, out_specs=out_specs, check_vma=False)
```

time: 75.5 us -> 68.7 us (0.910)
  Pallas kernels: 74.7 us -> 67.9 us
    pallas_call x2, Pallas kernels: 74.7 us -> 67.9 us  [the longest x1 66.5 us: layer(): pl.pallas_call(functools.partial(layer_kernel, n_ep, n_tp, pad_slot, taps...]
where the time goes in v2:
time: 68.7 us; the launch traced here: 68.5 us
  Pallas kernels  67.9 us (99%)
    pallas_call x1, Pallas kernels, layer(): pl.pallas_call(functools.partial(layer_kernel, n_ep, n_tp, pad_slot, taps...  66.5 us

profile of v2, /device:TPU:0, one launch (start us, length us, event | category | flops | bytes accessed | tf_op | source)
XLA Modules:
  0.0 68.5 jit_solution(1640034109853959432)
XLA Ops:
  0.6 66.5 %shard_map.140 = (bf16[256,2048]{1,0:T(8,128)(2,1)S(1)}, bf16[256,2048]{1,0:T(8,128)(2,1)S(1)}, bf16[256,256]{1,0:T(8,128)(2,1)S(1)}) custom-call(bf16[1024,256]{1,0:T(8,128)(2,1)} %og_hbm.1, bf16[1024,256]{1,0:T(8,128)(2,1)} %ig_hbm.1, bf16[1024,256]{1,0:T(8,128)(2,1)} %ci_hbm.1, f32[3,256]{1,0:T(4,128)} %taps_hbm.1, f32[1,256]{1,0:T(1,128)} %bitcast.7, ...), custom_call_target="tpu_custom_call" | custom-call | flops 6442450944 | bytes 16777216 | tf_op jit(solution)/shard_map/pallas_call | solution.py:401
  67.2 1.4 %shard_map.141 = (bf16[256,2048]{1,0:T(8,128)(2,1)}, bf16[256,2048]{1,0:T(8,128)(2,1)}) custom-call(bf16[256,2048]{1,0:T(8,128)(2,1)S(1)} %get-tuple-element.5.mixed_in, bf16[256,2048]{1,0:T(8,128)(2,1)S(1)} %get-tuple-element.6.fin, bf16[256,256]{1,0:T(8,128)(2,1)S(1)} %get-tuple-element.7.place), custom_call_target="tpu_custom_call" | custom-call | flops 268435456 | bytes 4194304 | tf_op jit(solution)/shard_map/pallas_call | solution.py:441

commit v3 on v2

--- a/solution.py
+++ b/solution.py
@@ -45,7 +45,7 @@
     x_hbm, mgain_hbm, ids_hbm, rw_hbm, wg_hbm, wu_hbm, wd_hbm,
     mixed, fin, place,
     og, ig, ci, taps, ggain, wm, x, mgain, ids, rw, wg, wu, wd,
-    normed, gated, norm, sorted_rows, landed, picked, xin, hidden, comb, sums, mixin,
+    normed, gated, raw, sorted_rows, landed, picked, xin, hidden, comb, sums, mixin,
     in_sem, h_send, h_recv, m_send, m_recv, d_send, d_recv, p_send, p_recv, r_send, r_recv, f_send, f_recv,
 ):
     me_e = lax.axis_index("ep")
@@ -57,6 +57,21 @@
     rows_a, lanes = og.shape
     part = rows_a // n_tp
     quarter = n_ep // 4
+    q0, q1, q2, q3 = [list(range(i * quarter, (i + 1) * quarter)) for i in range(4)]
+
+    middle = ((me_e // quarter + 1) // 2) % 2
+    split = quarter // 2
+    leaving = q1 + q0 + q2 + q3, q2 + q0 + q1 + q3
+    coming = q0 + q2[:split] + q1 + q2[split:] + q3, q0 + q1 + q2 + q3
+
+    def pick(orders, step, of=lambda k: k):
+        outer, inner = orders[0][step], orders[1][step]
+        if outer == inner:
+            return of(outer)
+        return middle * of(inner) + (1 - middle) * of(outer)
+
+    def peer(k):
+        return flip(me_e, k)
 
     barrier = pltpu.get_barrier_semaphore()
     for k in range(1, n_ep):
@@ -109,22 +124,24 @@
 
     loads["mgain"].wait()
     loads["x"].wait()
-    step = 32
-
-    @pl.loop(0, tok // step)
-    def _(i):
-        at = pl.ds(pl.multiple_of(i * step, step), step)
-        wide = x[at, :].astype(F32)
-        scale = lax.rsqrt(jnp.mean(wide * wide, axis=-1, keepdims=True) + 1e-06)
-        norm[at, :] = (wide * scale * mgain[...]).astype(BF16)
 
     @pl.loop(0, width // 512)
     def _(f):
         cols = pl.ds(pl.multiple_of(f * 512, 512), 512)
-        sorted_rows[:, cols] = jnp.dot(
-            place[...], norm[:, cols], preferred_element_type=F32
-        ).astype(BF16)
-
+        raw[:, cols] = jnp.dot(place[...], x[:, cols], preferred_element_type=F32).astype(BF16)
+
+    def rows_of(ep):
+        return pl.ds(pl.multiple_of(ep * rows, rows), rows)
+
+    def normalize(block):
+        wide = raw[block, :].astype(F32)
+        scale = lax.rsqrt(jnp.mean(wide * wide, axis=-1, keepdims=True) + 1e-06)
+        sorted_rows[block, 0:width] = (wide * scale * mgain[...]).astype(BF16)
+
+    def prepare(step):
+        normalize(rows_of(pick(leaving, step, peer)))
+
+    prepare(0)
     pl.semaphore_wait(barrier, n_ep - 1 + n_tp - 1)
 
     others = pl.ds(0, (n_tp - 1) * pad_slot)
@@ -156,32 +173,28 @@
         for copy in halos:
             copy.start()
 
-    dispatch = {}
-    for k in range(1, n_ep):
-        to = flip(me_e, k)
-        dispatch[k] = send(
-            sorted_rows.at[pl.ds(pl.multiple_of(to * rows, rows), rows)],
-            landed.at[k], d_send, d_recv.at[k], to, me_t,
-        )
-    landed[0] = sorted_rows[pl.ds(pl.multiple_of(me_e * rows, rows), rows), :]
-
-    def scatter(k):
-        if k:
-            dispatch[k].wait_recv()
+    def depart(step):
+        to, slot = pick(leaving, step, peer), pick(leaving, step)
+        send(sorted_rows.at[rows_of(to)], landed.at[slot], d_send, d_recv.at[slot], to, me_t)
+
+    def scatter(step):
+        k = pick(coming, step)
+        if step:
+            settle(d_recv.at[k], landed.at[k])
         chosen = (landed[k, :, pl.ds(width, slots)].astype(F32) != 0.0).astype(BF16)
         picked[k] = tdot(chosen, landed[k, :, 0:width]).astype(BF16)
+
+        def cell(j):
+            return pl.ds(pl.multiple_of((k * n_tp + j) * pad_slot, pad_slot), pad_slot)
+
         for j in range(n_tp - 1, 0, -1):
             to = flip(me_t, j)
             send(
                 picked.at[k, pl.ds(pl.multiple_of(to * pad_slot, pad_slot), pad_slot)],
-                xin.at[pl.ds((k * n_tp + j) * pad_slot, pad_slot)],
-                p_send, p_recv.at[k // quarter], me_e, to,
+                xin.at[cell(j)], p_send, p_recv.at[k // quarter], me_e, to,
             )
-        xin[pl.ds(k * n_tp * pad_slot, pad_slot), :] = picked[
-            k, pl.ds(pl.multiple_of(me_t * pad_slot, pad_slot), pad_slot), :
-        ]
-
-    own_lanes = pl.ds(pl.multiple_of(me_t * lanes, lanes), lanes)
+        xin[cell(0), :] = picked[k, pl.ds(pl.multiple_of(me_t * pad_slot, pad_slot), pad_slot), :]
+
 
     def conv_ready():
         for name in ("og", "taps", "ggain"):
@@ -229,29 +242,36 @@
         if j:
             normed[pl.ds(base, part), :] = done
         else:
-            mixin[:, own_lanes] = done
+            mixin[0] = done
 
     def mix_send(j):
         to = flip(me_t, j)
         send(
-            normed.at[pl.ds(pl.multiple_of(to * part, part), part)], mixin.at[:, own_lanes],
+            normed.at[pl.ds(pl.multiple_of(to * part, part), part)], mixin.at[j],
             m_send, m_recv, me_e, to,
         )
 
     def mixer():
-        settle(m_recv, mixin.at[:, pl.ds(0, (n_tp - 1) * lanes)])
+        settle(m_recv, mixin.at[pl.ds(1, n_tp - 1)])
 
         @pl.loop(0, width // 512)
         def _(f):
             cols = pl.ds(pl.multiple_of(f * 512, 512), 512)
-            mixed[:, cols] = jnp.dot(mixin[...], wm[:, cols], preferred_element_type=F32).astype(BF16)
+            total = jnp.zeros((part, 512), F32)
+            for j in range(n_tp):
+                depth = pl.ds(pl.multiple_of(flip(me_t, j) * lanes, lanes), lanes)
+                total = total + jnp.dot(mixin[j], wm[depth, cols], preferred_element_type=F32)
+            mixed[:, cols] = total.astype(BF16)
 
     hid = wg.shape[1]
     mine = pl.ds(pl.multiple_of(me_t * pad_slot, pad_slot), pad_slot)
     here = pl.ds(pl.multiple_of(me_e * rows, rows), rows)
 
-    def expert(first, count):
-        settle(p_recv.at[first // quarter], xin.at[pl.ds(first * slots, count * (n_tp - 1) * pad_slot)])
+    def rows_in(ks):
+        settle(p_recv.at[ks[0] // quarter], xin.at[pl.ds(ks[0] * slots, len(ks) * (n_tp - 1) * pad_slot)])
+
+    def expert(ks):
+        first, count = ks[0], len(ks)
         span = pl.ds(first * slots, count * slots)
         hid_rows = pl.ds(0, count * slots)
 
@@ -269,8 +289,8 @@
                 hidden[hid_rows, :], wd[:, cols], preferred_element_type=F32
             ).astype(BF16)
 
-    def give_back(first, count):
-        for k in range(first, first + count):
+    def give_back(ks):
+        for k in ks:
             for j in range(n_tp - 1, 0, -1):
                 send(
                     xin.at[pl.ds((k * n_tp + j) * pad_slot, pad_slot)],
@@ -293,37 +313,71 @@
         send(sums.at[k], fin.at[here], f_send, f_recv, flip(me_e, k), me_t)
 
     half = n_ep // 2
-    scatter(0)
+    depart(0)
+    for step in range(1, n_ep):
+        prepare(step)
+        if step == quarter:
+            landed[0] = sorted_rows[rows_of(me_e), :]
+            scatter(0)
+        else:
+            depart(step)
     conv_ready()
-    for j in range(n_tp - 1, 0, -1):
+    conv(n_tp - 1)
+    mix_send(n_tp - 1)
+    for j in range(n_tp - 2, -1, -1):
         conv(j)
+    mix_send(1)
+    for k in q0[1:]:
+        scatter(k)
+    for k in q1[:split]:
+        scatter(k)
+    for k in q1[split:]:
+        scatter(k)
+    for k in q2[:split]:
+        scatter(k)
+    for name in ("wg", "wu", "wd"):
+        loads[name].wait()
+    rows_in(q0)
+    for k in q2[split:]:
+        scatter(k)
+    for j in range(n_tp - 2, 1, -1):
         mix_send(j)
-    conv(0)
-    for k in range(1, half):
-        scatter(k)
+    rows_in(q2)
+    for k in q3[:split]:
+        scatter(k)
+    expert(q2)
+    give_back(q2[:split])
+    rows_in(q1)
+    for k in q3[split:]:
+        scatter(k)
+    give_back(q2[split:])
+    expert(q1)
+    give_back(q1[split:])
+    for k in q2[:split]:
+        combine(k)
     loads["wm"].wait()
     mixer()
-    for name in ("wg", "wu", "wd"):
-        loads[name].wait()
-    for k in range(half, half + quarter):
-        scatter(k)
-    expert(0, quarter)
-    for k in range(half + quarter, n_ep):
-        scatter(k)
-    expert(half, quarter)
-    give_back(half, quarter)
-    expert(half + quarter, quarter)
-    give_back(half + quarter, quarter)
-    for k in range(half, half + quarter):
-        combine(k)
-    expert(quarter, quarter)
-    give_back(quarter, quarter)
-    give_back(0, quarter)
-    for k in range(half + quarter, n_ep):
-        combine(k)
-    for k in range(half - 1, quarter - 1, -1):
-        combine(k)
-    for k in range(quarter - 1, -1, -1):
+    rows_in(q3)
+    expert(q3)
+    for k in q2[split:]:
+        combine(k)
+    give_back(q3[split:])
+    for k in q1[split:]:
+        combine(k)
+    give_back(q1[:split])
+    give_back(q3[:split])
+    for k in q3[split:]:
+        combine(k)
+    expert(q0)
+    give_back(q0[split:])
+    for k in q1[:split]:
+        combine(k)
+    give_back(q0[:split])
+    for k in q3[:split]:
+        combine(k)
+    for k in q0[split:]:
+        combine(k)
+    for k in q0[:split]:
         combine(k)
     settle(f_recv, fin.at[pl.ds(0, (n_ep - 1) * rows)])
     @pl.when(me_e < n_ep - 1)
@@ -380,7 +434,7 @@
         vm((total // 4, hid), BF16),
         vm((n_ep, slots, width), BF16),
         vm((n_ep, rows, width), BF16),
-        vm((part, channels), BF16),
+        vm((n_tp, part, lanes), BF16),
         dma((13,)),
         dma(()),
         dma(()),

time: 68.7 us -> 65.8 us (0.958)
  Pallas kernels: 67.9 us -> 65 us
    pallas_call x1, Pallas kernels: 66.5 us -> 63.7 us  [layer(): pl.pallas_call(functools.partial(layer_kernel, n_ep, n_tp, pad_slot, taps...]
where the time goes in v3:
time: 65.8 us; the launch traced here: 65.7 us
  Pallas kernels  65 us (99%)
    pallas_call x1, Pallas kernels, layer(): pl.pallas_call(functools.partial(layer_kernel, n_ep, n_tp, pad_slot, taps...  63.7 us
    pallas_call x1, Pallas kernels, shards(): pl.pallas_call(finish_kernel, out_shape=[jax.ShapeDtypeStruct(mixed.shape...  1.35 us

profile of v3, /device:TPU:0, one launch (start us, length us, event | category | flops | bytes accessed | tf_op | source)
XLA Modules:
  0.0 65.7 jit_solution(9166257085348209223)
XLA Ops:
  0.6 63.7 %shard_map.140 = (bf16[256,2048]{1,0:T(8,128)(2,1)S(1)}, bf16[256,2048]{1,0:T(8,128)(2,1)S(1)}, bf16[256,256]{1,0:T(8,128)(2,1)S(1)}) custom-call(bf16[1024,256]{1,0:T(8,128)(2,1)} %og_hbm.1, bf16[1024,256]{1,0:T(8,128)(2,1)} %ig_hbm.1, bf16[1024,256]{1,0:T(8,128)(2,1)} %ci_hbm.1, f32[3,256]{1,0:T(4,128)} %taps_hbm.1, f32[1,256]{1,0:T(1,128)} %bitcast.7, ...), custom_call_target="tpu_custom_call" | custom-call | flops 6442450944 | bytes 16777216 | tf_op jit(solution)/shard_map/pallas_call | solution.py:455
  64.3 1.4 %shard_map.141 = (bf16[256,2048]{1,0:T(8,128)(2,1)}, bf16[256,2048]{1,0:T(8,128)(2,1)}) custom-call(bf16[256,2048]{1,0:T(8,128)(2,1)S(1)} %get-tuple-element.5.mixed_in, bf16[256,2048]{1,0:T(8,128)(2,1)S(1)} %get-tuple-element.6.fin, bf16[256,256]{1,0:T(8,128)(2,1)S(1)} %get-tuple-element.7.place), custom_call_target="tpu_custom_call" | custom-call | flops 268435456 | bytes 4194304 | tf_op jit(solution)/shard_map/pallas_call | solution.py:495

commit v4 on v3

--- a/solution.py
+++ b/solution.py
@@ -254,9 +254,8 @@
     def mixer():
         settle(m_recv, mixin.at[pl.ds(1, n_tp - 1)])
 
-        @pl.loop(0, width // 512)
-        def _(f):
-            cols = pl.ds(pl.multiple_of(f * 512, 512), 512)
+        for f in range(width // 512):
+            cols = pl.ds(f * 512, 512)
             total = jnp.zeros((part, 512), F32)
             for j in range(n_tp):
                 depth = pl.ds(pl.multiple_of(flip(me_t, j) * lanes, lanes), lanes)
@@ -275,16 +274,14 @@
         span = pl.ds(first * slots, count * slots)
         hid_rows = pl.ds(0, count * slots)
 
-        @pl.loop(0, hid // 256)
-        def _(f):
-            cols = pl.ds(pl.multiple_of(f * 256, 256), 256)
+        for f in range(hid // 256):
+            cols = pl.ds(f * 256, 256)
             gate = jnp.dot(xin[span, :], wg[:, cols], preferred_element_type=F32)
             up = jnp.dot(xin[span, :], wu[:, cols], preferred_element_type=F32)
             hidden[hid_rows, cols] = (gate / (1.0 + jnp.exp(-gate)) * up).astype(BF16)
 
-        @pl.loop(0, width // 512)
-        def _(f):
-            cols = pl.ds(pl.multiple_of(f * 512, 512), 512)
+        for f in range(width // 512):
+            cols = pl.ds(f * 512, 512)
             xin[span, cols] = jnp.dot(
                 hidden[hid_rows, :], wd[:, cols], preferred_element_type=F32
             ).astype(BF16)

time: 65.8 us -> 64.4 us (0.979)
  Pallas kernels: 65 us -> 63.6 us
    pallas_call x1, Pallas kernels: 63.7 us -> 62.2 us  [layer(): pl.pallas_call(functools.partial(layer_kernel, n_ep, n_tp, pad_slot, taps...]
where the time goes in v4:
time: 64.4 us; the launch traced here: 64.2 us
  Pallas kernels  63.6 us (99%)
    pallas_call x1, Pallas kernels, layer(): pl.pallas_call(functools.partial(layer_kernel, n_ep, n_tp, pad_slot, taps...  62.2 us
    pallas_call x1, Pallas kernels, shards(): pl.pallas_call(finish_kernel, out_shape=[jax.ShapeDtypeStruct(mixed.shape...  1.35 us

profile of v4, /device:TPU:0, one launch (start us, length us, event | category | flops | bytes accessed | tf_op | source)
XLA Modules:
  0.0 64.2 jit_solution(8223363347241214072)
XLA Ops:
  0.6 62.2 %shard_map.140 = (bf16[256,2048]{1,0:T(8,128)(2,1)S(1)}, bf16[256,2048]{1,0:T(8,128)(2,1)S(1)}, bf16[256,256]{1,0:T(8,128)(2,1)S(1)}) custom-call(bf16[1024,256]{1,0:T(8,128)(2,1)} %og_hbm.1, bf16[1024,256]{1,0:T(8,128)(2,1)} %ig_hbm.1, bf16[1024,256]{1,0:T(8,128)(2,1)} %ci_hbm.1, f32[3,256]{1,0:T(4,128)} %taps_hbm.1, f32[1,256]{1,0:T(1,128)} %bitcast.7, ...), custom_call_target="tpu_custom_call" | custom-call | flops 6442450944 | bytes 16777216 | tf_op jit(solution)/shard_map/pallas_call | solution.py:452
  62.9 1.4 %shard_map.141 = (bf16[256,2048]{1,0:T(8,128)(2,1)}, bf16[256,2048]{1,0:T(8,128)(2,1)}) custom-call(bf16[256,2048]{1,0:T(8,128)(2,1)S(1)} %get-tuple-element.5.mixed_in, bf16[256,2048]{1,0:T(8,128)(2,1)S(1)} %get-tuple-element.6.fin, bf16[256,256]{1,0:T(8,128)(2,1)S(1)} %get-tuple-element.7.place), custom_call_target="tpu_custom_call" | custom-call | flops 268435456 | bytes 4194304 | tf_op jit(solution)/shard_map/pallas_call | solution.py:492

commit v5 on v4

--- a/solution.py
+++ b/solution.py
@@ -141,7 +141,16 @@
     def prepare(step):
         normalize(rows_of(pick(leaving, step, peer)))
 
-    prepare(0)
+    normalize(rows_of(me_e))
+    landed[0] = sorted_rows[rows_of(me_e), :]
+
+    def sort_out(k):
+        chosen = (landed[k, :, pl.ds(width, slots)].astype(F32) != 0.0).astype(BF16)
+        picked[k] = tdot(chosen, landed[k, :, 0:width]).astype(BF16)
+
+    sort_out(0)
+    for step in range(quarter):
+        prepare(step)
     pl.semaphore_wait(barrier, n_ep - 1 + n_tp - 1)
 
     others = pl.ds(0, (n_tp - 1) * pad_slot)
@@ -181,8 +190,7 @@
         k = pick(coming, step)
         if step:
             settle(d_recv.at[k], landed.at[k])
-        chosen = (landed[k, :, pl.ds(width, slots)].astype(F32) != 0.0).astype(BF16)
-        picked[k] = tdot(chosen, landed[k, :, 0:width]).astype(BF16)
+            sort_out(k)
 
         def cell(j):
             return pl.ds(pl.multiple_of((k * n_tp + j) * pad_slot, pad_slot), pad_slot)
@@ -310,14 +318,12 @@
         send(sums.at[k], fin.at[here], f_send, f_recv, flip(me_e, k), me_t)
 
     half = n_ep // 2
-    depart(0)
-    for step in range(1, n_ep):
+    for step in range(quarter):
+        depart(step)
+    scatter(0)
+    for step in range(quarter + 1, n_ep):
         prepare(step)
-        if step == quarter:
-            landed[0] = sorted_rows[rows_of(me_e), :]
-            scatter(0)
-        else:
-            depart(step)
+        depart(step)
     conv_ready()
     conv(n_tp - 1)
     mix_send(n_tp - 1)
@@ -361,16 +367,16 @@
     give_back(q3[split:])
     for k in q1[split:]:
         combine(k)
+    give_back(q3[:split])
     give_back(q1[:split])
-    give_back(q3[:split])
     for k in q3[split:]:
         combine(k)
     expert(q0)
     give_back(q0[split:])
+    for k in q3[:split]:
+        combine(k)
+    give_back(q0[:split])
     for k in q1[:split]:
-        combine(k)
-    give_back(q0[:split])
-    for k in q3[:split]:
         combine(k)
     for k in q0[split:]:
         combine(k)

time: 64.4 us -> 64.4 us (level)
  no operation moved by 1% of the time
where the time goes in v5:
time: 64.4 us; the launch traced here: 64.2 us
  Pallas kernels  63.6 us (99%)
    pallas_call x1, Pallas kernels, layer(): pl.pallas_call(functools.partial(layer_kernel, n_ep, n_tp, pad_slot, taps...  62.2 us
    pallas_call x1, Pallas kernels, shards(): pl.pallas_call(finish_kernel, out_shape=[jax.ShapeDtypeStruct(mixed.shape...  1.35 us

profile of v5, /device:TPU:0, one launch (start us, length us, event | category | flops | bytes accessed | tf_op | source)
XLA Modules:
  0.0 64.2 jit_solution(9940256725354878790)
XLA Ops:
  0.6 62.2 %shard_map.140 = (bf16[256,2048]{1,0:T(8,128)(2,1)S(1)}, bf16[256,2048]{1,0:T(8,128)(2,1)S(1)}, bf16[256,256]{1,0:T(8,128)(2,1)S(1)}) custom-call(bf16[1024,256]{1,0:T(8,128)(2,1)} %og_hbm.1, bf16[1024,256]{1,0:T(8,128)(2,1)} %ig_hbm.1, bf16[1024,256]{1,0:T(8,128)(2,1)} %ci_hbm.1, f32[3,256]{1,0:T(4,128)} %taps_hbm.1, f32[1,256]{1,0:T(1,128)} %bitcast.7, ...), custom_call_target="tpu_custom_call" | custom-call | flops 6442450944 | bytes 16777216 | tf_op jit(solution)/shard_map/pallas_call | solution.py:458
  62.9 1.4 %shard_map.141 = (bf16[256,2048]{1,0:T(8,128)(2,1)}, bf16[256,2048]{1,0:T(8,128)(2,1)}) custom-call(bf16[256,2048]{1,0:T(8,128)(2,1)S(1)} %get-tuple-element.5.mixed_in, bf16[256,2048]{1,0:T(8,128)(2,1)S(1)} %get-tuple-element.6.fin, bf16[256,256]{1,0:T(8,128)(2,1)S(1)} %get-tuple-element.7.place), custom_call_target="tpu_custom_call" | custom-call | flops 268435456 | bytes 4194304 | tf_op jit(solution)/shard_map/pallas_call | solution.py:498
